TPU v7x, 128 devices: a whole 4x4x4 slice. The times are simulated.
128 devices in a mesh: sp: 16 (over z, y), tp: 8 (over x, core).
Axes of the slice: x: 4, y: 4, z: 4, core: 2. Of those that a mesh axis runs over, the one named last changes fastest.
Arguments:
- queries: bfloat16 [12288, 2048], P('sp', 'tp'), may hold values from -11 to 11
- key_rows: bfloat16 [12288, 2048], P('sp', 'tp'), may hold values from -4.5 to 4.5
- value_rows: bfloat16 [12288, 2048], P('sp', 'tp'), may hold values from -6 to 6
- log_forget: float32 [12288, 32], P('sp', 'tp'), may hold values from -1477.56 to 0, as said below
- stream_in: bfloat16 [12288, 2048], P('sp'), may hold values from -6 to 6
- out_weight: bfloat16 [2048, 2048], P('tp'), may hold values from -0.52734375 to 0.52734375
- mix_gain: float32 [2048], replicated, may hold values from 0.1 to 1.9
- mix_bias: float32 [2048], replicated, may hold values from -3 to 3
- gate_weight: bfloat16 [2048, 5632], P('sp', 'tp'), may hold values from -0.125 to 0.125
- up_weight: bfloat16 [2048, 5632], P('sp', 'tp'), may hold values from -0.125 to 0.125
- down_weight: bfloat16 [5632, 2048], P('tp', 'sp'), may hold values from -0.15917969 to 0.15917969
- ffn_gain: float32 [2048], replicated, may hold values from 0.1 to 1.9
- ffn_bias: float32 [2048], replicated, may hold values from -3 to 3
Outputs:
- layer_out: bfloat16 [12288, 2048], P(('sp', 'tp'))
Inputs may be any that keep to these rules, and one draw needn't show every extreme that they name: `log_forget`: each column never rises along the positions.
All inputs are finite; a program needn't handle non-finite values.
Results may differ from a plain program's by a relative error of at most 0.015.
Values may be sent and summed in bfloat16 or wider, within the bound.
A program may use at most 128 MiB of HBM per device.

v0:
```python
import jax
import jax.numpy as jnp
from jax import lax
from jax.sharding import PartitionSpec as P

ALPHA = 8.0**0.25
EPSILON = 1e-05


def laid_out(pieces, dim):
    lengths = list(pieces.shape[1:])
    lengths[dim] *= pieces.shape[0]
    return jnp.moveaxis(pieces, 0, dim).reshape(lengths)


def from_everyone(value, axis):
    copies = jnp.broadcast_to(value, (lax.axis_size(axis), *value.shape))
    return lax.all_to_all(copies, axis, split_axis=0, concat_axis=0, tiled=True)


def gathered_copies(value, axis, dim):
    return laid_out(from_everyone(value, axis), dim)


def in_one_piece(arrays, axis, dim, along):
    ends, at = ([], 0)
    for a in arrays[:-1]:
        at += a.shape[along]
        ends.append(at)
    both = jnp.concatenate(arrays, axis=along)
    return tuple(jnp.split(lax.all_gather(both, axis, axis=dim, tiled=True), ends, axis=along))


def in_blocks(value, dim, count):
    before, after = (value.shape[:dim], value.shape[dim + 1 :])
    return jnp.moveaxis(value.reshape(*before, count, -1, *after), dim, 0)


def sum_at_owner(value, axis, dim):
    pieces = in_blocks(value, dim, lax.axis_size(axis))
    arrived = lax.all_to_all(pieces, axis, split_axis=0, concat_axis=0, tiled=True)
    return arrived.astype(jnp.float32).sum(axis=0)


def layer_norm(matrix, norm_gain, norm_shift):
    centred = matrix - jnp.mean(matrix, axis=-1, keepdims=True)
    spread = jnp.mean(centred * centred, axis=-1, keepdims=True)
    return centred * lax.rsqrt(spread + EPSILON) * norm_gain + norm_shift


def attend(queries, key_rows, value_rows, log_forget):
    length, row_width = queries.shape
    head_count = log_forget.shape[1]
    head_dim = row_width // head_count
    score_scale = head_dim ** (-0.5)
    first_pos = lax.axis_index("sp") * length
    last_pos = first_pos + length
    query_heads = queries.reshape(length, head_count, head_dim)
    query_gates = log_forget.T
    query_pos = first_pos + jnp.arange(length, dtype=jnp.int32)
    gates_all = gathered_copies(log_forget, "sp", 0)
    initial = (
        jnp.full((head_count, length), -1e30, jnp.float32),
        jnp.zeros((head_count, length), jnp.float32),
        jnp.zeros((length, head_count, head_dim), jnp.float32),
    )
    running = initial
    key_piece, value_piece = in_one_piece((key_rows, value_rows), "sp", 0, 1)
    piece_len = key_piece.shape[0]
    shards = piece_len // length
    group_size = max(
        [
            count_try
            for count_try in range(1, shards + 1)
            if shards % count_try == 0 and count_try * length <= max(length, 512)
        ]
    )
    block_len = group_size * length
    blocks = piece_len // block_len
    key_blocks = key_piece.reshape(blocks, block_len, head_count, head_dim)
    value_blocks = value_piece.reshape(blocks, block_len, head_count, head_dim)
    gate_blocks = gates_all.reshape(blocks, block_len, head_count)
    block_starts = block_len * jnp.arange(blocks, dtype=jnp.int32)

    def one_block(running_state, packed):
        key_block, value_block, gate_block, block_start = packed

        def compute(state_in):
            highest, totals, weighted = state_in
            scores = (
                jnp.einsum(
                    "qhd,khd->hqk", query_heads, key_block, preferred_element_type=jnp.float32
                )
                * score_scale
            )
            scores = scores + query_gates[:, :, None] - gate_block.T[:, None, :]
            key_pos = block_start + jnp.arange(block_len, dtype=jnp.int32)
            allowed = (key_pos[None, :] <= query_pos[:, None])[None]
            masked = jnp.where(allowed, scores, -1e30)
            new_high = jnp.maximum(highest, jnp.max(masked, axis=2))
            weights = jnp.where(allowed, jnp.exp(masked - new_high[:, :, None]), 0.0)
            factor = jnp.exp(highest - new_high)
            totals = totals * factor + jnp.sum(weights, axis=2)
            weighted = weighted * factor.T[:, :, None] + jnp.einsum(
                "hqk,khd->qhd",
                weights.astype(jnp.bfloat16),
                value_block,
                preferred_element_type=jnp.float32,
            )
            return (new_high, totals, weighted)

        def keep_state(state_in):
            return state_in

        return (lax.cond(block_start < last_pos, compute, keep_state, running_state), None)

    running, unused = lax.scan(
        one_block, running, (key_blocks, value_blocks, gate_blocks, block_starts)
    )
    highest, totals, weighted = running
    return (weighted / totals.T[:, :, None]).reshape(length, row_width).astype(jnp.bfloat16)


def body(
    queries,
    key_rows,
    value_rows,
    log_forget,
    stream_in,
    out_weight,
    mix_gain,
    mix_bias,
    gate_weight,
    up_weight,
    down_weight,
    ffn_gain,
    ffn_bias,
):
    attended = attend(queries, key_rows, value_rows, log_forget)
    length = attended.shape[0]
    own_rows = length // lax.axis_size("tp")
    offset = lax.axis_index("tp") * own_rows
    summed = sum_at_owner(
        jnp.dot(attended, out_weight, preferred_element_type=jnp.float32).astype(jnp.bfloat16),
        "tp",
        0,
    )
    mix_out = lax.optimization_barrier(summed.astype(jnp.bfloat16)).astype(jnp.float32)
    stream_own = lax.dynamic_slice_in_dim(stream_in, offset, own_rows, 0)
    normed = layer_norm(
        ALPHA * stream_own.astype(jnp.float32) + mix_out, mix_gain, mix_bias
    ).astype(jnp.bfloat16)
    gathered = lax.all_gather(normed, "tp", axis=0, tiled=True)
    pieces = in_one_piece((gate_weight, up_weight), "sp", 0, 1)
    gate_part = jnp.dot(gathered, pieces[0], preferred_element_type=jnp.float32)
    up_part = jnp.dot(gathered, pieces[1], preferred_element_type=jnp.float32)
    hidden = (jax.nn.silu(gate_part) * up_part).astype(jnp.bfloat16)
    partial_terms = jnp.dot(
        hidden,
        lax.all_gather(down_weight, "sp", axis=1, tiled=True),
        preferred_element_type=jnp.float32,
    )
    lowered = lax.psum_scatter(
        partial_terms.astype(jnp.bfloat16), "tp", scatter_dimension=0, tiled=True
    ).astype(jnp.float32)
    lowered = lax.optimization_barrier(lowered.astype(jnp.bfloat16)).astype(jnp.float32)
    result = layer_norm(ALPHA * normed.astype(jnp.float32) + lowered, ffn_gain, ffn_bias)
    return result.astype(jnp.bfloat16)


def solution(mesh):
    placed = (
        P("sp", "tp"),
        P("sp", "tp"),
        P("sp", "tp"),
        P("sp", "tp"),
        P("sp", None),
        P("tp", None),
        P(),
        P(),
        P("sp", "tp"),
        P("sp", "tp"),
        P("tp", "sp"),
        P(),
        P(),
    )
    return jax.shard_map(
        body, mesh=mesh, in_specs=placed, out_specs=P(("sp", "tp"), None), check_vma=False
    )
```

profile of v0, /device:TPU:0, one launch (start us, length us, event | category | flops | bytes accessed | tf_op | source)
XLA Modules:
  0.0 604.3 jit_solution(4880820120093457124)
XLA Ops:
  6.5 2.2 pad_maximum_fusion
  8.8 1.8 pad_maximum_fusion.1
  10.6 1.4 broadcast_in_dim.56
  12.0 8.2 %all-to-all-start = ((f32[16,768,4]{1,2,0:T(4,128)}), f32[16,768,4]{1,2,0:T(4,128)S(1)}, u32[]{:S(2)}, u32[]{:S(2)}) async-start(f32[16,768,4]{1,2,0:T(4,128)} %broadcast_in_dim.56), calls=%async_computation | async-start | bytes 393216 | tf_op jit(solution)/shard_map/all_to_all | solution.py:18
  20.2 1.2 copy.18
  21.4 80.5 %all-gather.5.cloned.1.call-done = bf16[12288,512]{1,0:T(8,128)(2,1)} async-done(((bf16[768,512]{1,0:T(8,128)(2,1)}), bf16[12288,512]{1,0:T(8,128)(2,1)}) %all-gather.5.cloned.1.call-update) | async-done | bytes 12582928 | tf_op jit(solution)/shard_map/all_gather | solution.py:31
  101.9 10.1 %fusion.36 = (bf16[12288,256]{1,0:T(8,128)(2,1)}, bf16[12288,256]{1,0:T(8,128)(2,1)}) fusion(bf16[12288,512]{1,0:T(8,128)(2,1)} %all-gather.5.cloned.1.call-done), kind=kLoop, calls=%fused_computation.51 | loop fusion | bytes 25165824 | tf_op jit(solution)/shard_map/split | solution.py:31
  112.0 18.8 %reshape.82 = bf16[16,768,4,64]{3,2,1,0:T(4,128)(2,1)} reshape(bf16[12288,256]{1,0:T(8,128)(2,1)} %get-tuple-element.249) | data formatting | bytes 12582912 | tf_op jit(solution)/shard_map/reshape | solution.py:80
  130.8 18.1 %copy.20 = bf16[16,768,4,64]{1,3,2,0:T(8,128)(2,1)} copy(bf16[16,768,4,64]{3,2,1,0:T(4,128)(2,1)} %reshape.82) | data formatting | bytes 12582912
  148.9 18.8 %reshape.83 = bf16[16,768,4,64]{3,2,1,0:T(4,128)(2,1)} reshape(bf16[12288,256]{1,0:T(8,128)(2,1)} %get-tuple-element.248) | data formatting | bytes 12582912 | tf_op jit(solution)/shard_map/reshape | solution.py:81
  167.6 18.1 %copy.21 = bf16[16,768,4,64]{1,3,2,0:T(8,128)(2,1)} copy(bf16[16,768,4,64]{3,2,1,0:T(4,128)(2,1)} %reshape.83) | data formatting | bytes 12582912
  185.8 33.5 %while.15 = (s32[]{:T(128)}, f32[4,768]{1,0:T(4,128)S(1)}, f32[4,768]{1,0:T(4,128)S(1)}, f32[768,4,64]{0,2,1:T(8,128)S(1)}, s32[16]{0:T(128)S(1)}, /*index=5*/s3...) while((s32[]{:T(128)}, f32[4,768]{1,0:T(4,128)S(1)}, ...), condition=%wide.region_5.6_spmd.clone, body=%wide.region_0.5_spmd.clone.sunk | while | flops 649800192 | bytes 33738040 | solution.py:117
  185.8 0.6 dynamic_slice.50
  187.1 13.1 %conditional.3 = ((f32[4,768]{1,0:T(4,128)S(1)}, f32[4,768]{1,0:T(4,128)S(1)}, f32[768,4,64]{0,2,1:T(8,128)S(1)})) conditional(s32[]{:T(128)} %convert_element_type.100, (f32[4,768]{1,0:T(4,128)S(1)}, f32[4,768]{1,0:T(4,128)S(1)}, f32[768,4,64]{0,2,1:T(8,128)S(1)}) %tuple.41, (s32[]{:T(128)}, s32[]{:T(128)}, bf16[16,768,4,64]{1,3,2,0:T(8,128)(2,1)}, ...), branch_computations={%region_1.1_spmd, %region_2.4_spmd} | conditional | flops 649800192 | bytes 33734700 | solution.py:115
  187.1 0.7 iota_add_fusion
  188.2 3.9 fusion.4
  192.0 4.6 fusion.11
  196.6 3.5 fusion.3
  200.2 0.6 dynamic_slice.50
  201.4 0.6 dynamic_slice.50
  202.7 0.6 dynamic_slice.50
  204.0 0.6 dynamic_slice.50
  205.3 0.6 dynamic_slice.50
  206.5 0.6 dynamic_slice.50
  207.8 0.6 dynamic_slice.50
  209.1 0.6 dynamic_slice.50
  210.4 0.6 dynamic_slice.50
  211.7 0.6 dynamic_slice.50
  212.9 0.6 dynamic_slice.50
  214.2 0.6 dynamic_slice.50
  215.5 0.6 dynamic_slice.50
  216.8 0.6 dynamic_slice.50
  218.0 0.6 dynamic_slice.50
  219.4 2.7 convolution_convert_fusion.1
  222.1 4.6 all-to-all-start.1
  226.9 38.2 %all-to-all-done.1 = bf16[8,96,2048]{2,1,0:T(8,128)(2,1)} async-done(((bf16[8,96,2048]{2,1,0:T(8,128)(2,1)}), bf16[8,96,2048]{2,1,0:T(8,128)(2,1)}, u32[]{:S(2)}, u32[]{:S(2)}) %all-to-all-start.1) | async-done | bytes 3145760 | tf_op jit(solution)/shard_map/all_to_all | solution.py:41
  265.1 2.5 reduce_sum.59
  267.6 1.2 fusion.33
  268.8 1.3 multiply_reduce_fusion.1
  270.2 2.0 add_convert_fusion.1
  272.8 220.0 %all-gather.7.cloned.1.call-done = bf16[768,2048]{1,0:T(8,128)(2,1)} async-done(((bf16[96,2048]{1,0:T(8,128)(2,1)}), bf16[768,2048]{1,0:T(8,128)(2,1)}) %all-gather.7.cloned.1.call-update) | async-done | bytes 3145744 | tf_op jit(solution)/shard_map/all_gather | solution.py:153
  492.8 6.5 %fusion.27 = f32[768,704]{0,1:T(8,128)} fusion(bf16[768,2048]{1,0:T(8,128)(2,1)} %all-gather.7.cloned.1.call-done, bf16[2048,1408]{0,1:T(8,128)(2,1)} %all-gather.9.cloned.1.call-done), kind=kOutput, calls=%fused_computation.31 | convolution fusion | flops 2214592512 | bytes 8192000 | tf_op jit(solution)/shard_map/dot_general | solution.py:155
  499.3 46.2 %all-gather.11.cloned.1.call-done = bf16[704,2048]{1,0:T(8,128)(2,1)} async-done(((bf16[704,128]{1,0:T(8,128)(2,1)}), bf16[704,2048]{1,0:T(8,128)(2,1)}) %all-gather.11.cloned.1.call-update) | async-done | bytes 2883600 | tf_op jit(solution)/shard_map/all_gather | solution.py:160
  545.5 12.4 %convolution_convert_fusion = bf16[768,2048]{1,0:T(8,128)(2,1)} fusion(bf16[704,2048]{1,0:T(8,128)(2,1)} %all-gather.11.cloned.1.call-done, f32[768,704]{0,1:T(8,128)} %fusion.27, bf16[768,2048]{1,0:T(8,128)(2,1)} %all-gather.7.cloned.1.call-done, bf16[2048,1408]{0,1:T(8,128)(2,1)} %all-gather.9.cloned.1.call-done), kind=kOutput, calls=%fused_computation.27 | convolution fusion | flops 4434001920 | bytes 14221312 | tf_op jit(solution)/shard_map/dot_general | solution.py:158
  557.9 35.3 %reduce-scatter.2.cloned.1.call-done = bf16[96,2048]{1,0:T(8,128)(2,1)} async-done(((bf16[768,2048]{1,0:T(8,128)(2,1)}), bf16[96,2048]{1,0:T(8,128)(2,1)}) %reduce-scatter.2.cloned.1.call-update) | async-done | bytes 393232 | tf_op jit(solution)/shard_map/reduce_scatter | solution.py:163
  593.2 1.2 fusion.34
  594.4 1.3 multiply_reduce_fusion
  595.7 2.0 add_convert_fusion
  (71 shorter events, 1.8 us)
Async XLA Ops:
  6.5 212.9 %copy-start = (bf16[256,2048]{1,0:T(8,128)(2,1)S(1)}, bf16[256,2048]{1,0:T(8,128)(2,1)}, u32[]{:S(2)}) copy-start(bf16[256,2048]{1,0:T(8,128)(2,1)} %param.22) | copy-start | bytes 3145732
  6.5 95.4 %all-gather.5.cloned.1.call-start = ((), (), s32[]{:S(2)}) async-start(), calls=%async_computation.3 | async-start | bytes 13369344 | tf_op jit(solution)/shard_map/all_gather | solution.py:31
  8.8 264.1 %all-gather.9.cloned.1.call-start = ((), (), s32[]{:S(2)}) async-start(), calls=%async_computation.5 | async-start | bytes 6127616 | tf_op jit(solution)/shard_map/all_gather | solution.py:31
  12.0 173.7 %all-to-all-start = ((f32[16,768,4]{1,2,0:T(4,128)}), f32[16,768,4]{1,2,0:T(4,128)S(1)}, u32[]{:S(2)}, u32[]{:S(2)}) async-start(f32[16,768,4]{1,2,0:T(4,128)} %broadcast_in_dim.56), calls=%async_computation | async-start | bytes 393216 | tf_op jit(solution)/shard_map/all_to_all | solution.py:18
  167.6 18.2 %copy-start.2 = (f32[768,4]{0,1:T(4,128)S(1)}, f32[768,4]{0,1:T(4,128)}, u32[]{:S(2)}) copy-start(f32[768,4]{0,1:T(4,128)} %param.20) | copy-start | bytes 36868
  222.1 48.0 %copy-start.3 = (f32[2048]{0:T(1024)S(1)}, f32[2048]{0:T(1024)}, u32[]{:S(2)}) copy-start(f32[2048]{0:T(1024)} %param.24) | copy-start | bytes 24580
  222.1 48.0 %copy-start.4 = (f32[2048]{0:T(1024)S(1)}, f32[2048]{0:T(1024)}, u32[]{:S(2)}) copy-start(f32[2048]{0:T(1024)} %param.23) | copy-start | bytes 24580
  222.1 43.0 %all-to-all-start.1 = ((bf16[8,96,2048]{2,1,0:T(8,128)(2,1)}), bf16[8,96,2048]{2,1,0:T(8,128)(2,1)}, u32[]{:S(2)}, u32[]{:S(2)}) async-start(bf16[8,96,2048]{2,1,0:T(8,128)(2,1)} %bitcast.45), calls=%async_computation.1 | async-start | bytes 6291456 | tf_op jit(solution)/shard_map/all_to_all | solution.py:41
  226.7 266.1 %all-gather.7.cloned.1.call-start = ((), (), s32[]{:S(2)}) async-start(), calls=%async_computation.4 | async-start | bytes 3538944 | tf_op jit(solution)/shard_map/all_gather | solution.py:153
  272.2 273.3 %all-gather.11.cloned.1.call-start = ((), (), s32[]{:S(2)}) async-start(), calls=%async_computation.6 | async-start | bytes 3063808 | tf_op jit(solution)/shard_map/all_gather | solution.py:160
  272.8 320.4 %reduce-scatter.2.cloned.1.call-start = ((), (), s32[]{:S(2)}) async-start(), calls=%async_computation.7 | async-start | bytes 3538944 | tf_op jit(solution)/shard_map/reduce_scatter | solution.py:163
  499.3 93.9 %copy-start.1 = (bf16[96,2048]{1,0:T(8,128)(2,1)S(1)}, bf16[96,2048]{1,0:T(8,128)(2,1)}, u32[]{:S(2)}) copy-start(bf16[96,2048]{1,0:T(8,128)(2,1)} %add_convert_fusion.1) | copy-start | bytes 1179652
  499.3 96.4 %copy-start.5 = (f32[2048]{0:T(1024)S(1)}, f32[2048]{0:T(1024)}, u32[]{:S(2)}) copy-start(f32[2048]{0:T(1024)} %param.29) | copy-start | bytes 24580
  499.3 96.4 %copy-start.6 = (f32[2048]{0:T(1024)S(1)}, f32[2048]{0:T(1024)}, u32[]{:S(2)}) copy-start(f32[2048]{0:T(1024)} %param.28) | copy-start | bytes 24580
Sparse Core Ops, SparseCore 0:
  9.5 92.3 all-gather.4
  104.0 64.0 all-gather.8
  272.3 220.4 all-gather.6
  494.8 50.6 all-gather.10
  558.0 35.0 reduce-scatter.1
where the time goes:
time: 608 us; the launch traced here: 604 us
  waiting for transfers between devices  421 us (69%)
  local copies, waits for them, and re-layouts  95.9 us (16%)
  matrix products  30.1 us (5%)
  other arithmetic  20.1 us (3%)
  between operations  13.3 us (2%)
  starting transfers between devices  13.1 us (2%)
  loops' own time  11.1 us (2%)
    all_gather x1, waiting for transfers between devices, body(): gathered = lax.all_gather(normed, 'tp', axis=0, tiled=True)  220 us
    all_gather x2, waiting for transfers between devices, in_one_piece(): lax.all_gather(both, axis, axis=dim, tiled=True)  80.5 us
    all_gather x1, waiting for transfers between devices, body(): lax.all_gather(down_weight, 'sp', axis=1, tiled=True)  46.2 us
    all_to_all x1, waiting for transfers between devices, sum_at_owner(): lax.all_to_all(pieces, axis, split_axis=0, concat_axis=0, tiled=True)  38.2 us
    unnamed x17, local copies, waits for them, and re-layouts  37.4 us
    reduce_scatter x1, waiting for transfers between devices, body(): lax.psum_scatter(partial_terms.astype(jnp.bfloat16), 'tp', scatter_dimens...  35.3 us
    reshape x1, local copies, waits for them, and re-layouts, attend(): key_blocks = key_piece.reshape(blocks, block_len, head_count, head_dim)  18.8 us
    reshape x1, local copies, waits for them, and re-layouts, attend(): value_blocks = value_piece.reshape(blocks, block_len, head_count, head_dim)  18.8 us
  transfers between devices with their start and end apart: 7, of which 5 were waited for; matrix products, arithmetic and copies ran while one was open for 21% of the time, Pallas kernels for 0%

commit v1 on v0

--- a/solution.py
+++ b/solution.py
@@ -5,6 +5,12 @@
 
 ALPHA = 8.0**0.25
 EPSILON = 1e-05
+
+
+def all_parts(shard, mesh_axis, d):
+    parts = lax.all_gather(shard, mesh_axis, axis=0, tiled=False)
+    full = jnp.concatenate(parts, axis=d)
+    return full
 
 
 def laid_out(pieces, dim):
@@ -156,9 +162,7 @@
     up_part = jnp.dot(gathered, pieces[1], preferred_element_type=jnp.float32)
     hidden = (jax.nn.silu(gate_part) * up_part).astype(jnp.bfloat16)
     partial_terms = jnp.dot(
-        hidden,
-        lax.all_gather(down_weight, "sp", axis=1, tiled=True),
-        preferred_element_type=jnp.float32,
+        hidden, all_parts(down_weight, "sp", 1), preferred_element_type=jnp.float32
     )
     lowered = lax.psum_scatter(
         partial_terms.astype(jnp.bfloat16), "tp", scatter_dimension=0, tiled=True

time: 608 us -> 563 us (0.926)
  waiting for transfers between devices: 421 us -> 371 us
    all_gather x1, waiting for transfers between devices: 46.2 us -> 0.02 us  [all_parts(): parts = lax.all_gather(shard, mesh_axis, axis=0, tiled=False)]
  transfers between devices with their start and end apart: 7 -> 7, of which waited for: 5 -> 4; matrix products, arithmetic and copies ran while one was open for 21% -> 22% of each run, Pallas kernels for 0% -> 0%
where the time goes in v1:
time: 563 us; the launch traced here: 560 us
  waiting for transfers between devices  371 us (66%)
  local copies, waits for them, and re-layouts  101 us (18%)
  matrix products  30.2 us (5%)
  other arithmetic  20.1 us (4%)
  between operations  13.3 us (2%)
  starting transfers between devices  13.1 us (2%)
  loops' own time  11.1 us (2%)
    all_gather x1, waiting for transfers between devices, body(): gathered = lax.all_gather(normed, 'tp', axis=0, tiled=True)  215 us
    all_gather x2, waiting for transfers between devices, in_one_piece(): lax.all_gather(both, axis, axis=dim, tiled=True)  80.2 us
    all_to_all x1, waiting for transfers between devices, sum_at_owner(): lax.all_to_all(pieces, axis, split_axis=0, concat_axis=0, tiled=True)  38.2 us
    unnamed x17, local copies, waits for them, and re-layouts  37.5 us
    reduce_scatter x1, waiting for transfers between devices, body(): lax.psum_scatter(partial_terms.astype(jnp.bfloat16), 'tp', scatter_dimens...  36.1 us
    reshape x1, local copies, waits for them, and re-layouts, attend(): value_blocks = value_piece.reshape(blocks, block_len, head_count, head_dim)  18.7 us
    reshape x1, local copies, waits for them, and re-layouts, attend(): key_blocks = key_piece.reshape(blocks, block_len, head_count, head_dim)  18.7 us
    dot_general x1, matrix products, body(): jnp.dot(hidden, all_parts(down_weight, 'sp', 1), preferred_element_type=j...  12.5 us
  transfers between devices with their start and end apart: 7, of which 4 were waited for; matrix products, arithmetic and copies ran while one was open for 22% of the time, Pallas kernels for 0%

profile of v1, /device:TPU:0, one launch (start us, length us, event | category | flops | bytes accessed | tf_op | source)
XLA Modules:
  0.0 559.6 jit_solution(8461673568694545739)
XLA Ops:
  6.5 2.2 pad_maximum_fusion
  8.8 0.7 all-gather.12.cloned.1.call-update
  9.6 1.8 pad_maximum_fusion.1
  11.3 1.4 broadcast_in_dim.56
  12.8 8.2 %all-to-all-start = ((f32[16,768,4]{1,2,0:T(4,128)}), f32[16,768,4]{1,2,0:T(4,128)S(1)}, u32[]{:S(2)}, u32[]{:S(2)}) async-start(f32[16,768,4]{1,2,0:T(4,128)} %broadcast_in_dim.56), calls=%async_computation | async-start | bytes 393216 | tf_op jit(solution)/shard_map/all_to_all | solution.py:24
  20.9 1.2 copy.18
  22.2 80.2 %all-gather.6.cloned.1.call-done = bf16[12288,512]{1,0:T(8,128)(2,1)} async-done(((bf16[768,512]{1,0:T(8,128)(2,1)}), bf16[12288,512]{1,0:T(8,128)(2,1)}) %all-gather.6.cloned.1.call-update) | async-done | bytes 12582928 | tf_op jit(solution)/shard_map/all_gather | solution.py:37
  102.4 10.1 %fusion.38 = (bf16[12288,256]{1,0:T(8,128)(2,1)}, bf16[12288,256]{1,0:T(8,128)(2,1)}) fusion(bf16[12288,512]{1,0:T(8,128)(2,1)} %all-gather.6.cloned.1.call-done), kind=kLoop, calls=%fused_computation.53 | loop fusion | bytes 25165824 | tf_op jit(solution)/shard_map/split | solution.py:37
  112.5 18.7 %reshape.91 = bf16[16,768,4,64]{3,2,1,0:T(4,128)(2,1)} reshape(bf16[12288,256]{1,0:T(8,128)(2,1)} %get-tuple-element.249) | data formatting | bytes 12582912 | tf_op jit(solution)/shard_map/reshape | solution.py:86
  131.1 18.2 %copy.20 = bf16[16,768,4,64]{1,3,2,0:T(8,128)(2,1)} copy(bf16[16,768,4,64]{3,2,1,0:T(4,128)(2,1)} %reshape.91) | data formatting | bytes 12582912
  149.3 18.7 %reshape.92 = bf16[16,768,4,64]{3,2,1,0:T(4,128)(2,1)} reshape(bf16[12288,256]{1,0:T(8,128)(2,1)} %get-tuple-element.248) | data formatting | bytes 12582912 | tf_op jit(solution)/shard_map/reshape | solution.py:87
  168.0 18.1 %copy.21 = bf16[16,768,4,64]{1,3,2,0:T(8,128)(2,1)} copy(bf16[16,768,4,64]{3,2,1,0:T(4,128)(2,1)} %reshape.92) | data formatting | bytes 12582912
  186.3 33.5 %while.15 = (s32[]{:T(128)}, f32[4,768]{1,0:T(4,128)S(1)}, f32[4,768]{1,0:T(4,128)S(1)}, f32[768,4,64]{0,2,1:T(8,128)S(1)}, s32[16]{0:T(128)S(1)}, /*index=5*/s3...) while((s32[]{:T(128)}, f32[4,768]{1,0:T(4,128)S(1)}, ...), condition=%wide.region_5.6_spmd.clone, body=%wide.region_0.5_spmd.clone.sunk | while | flops 649800192 | bytes 33738040 | solution.py:123
  186.3 0.6 dynamic_slice.50
  187.5 13.1 %conditional.3 = ((f32[4,768]{1,0:T(4,128)S(1)}, f32[4,768]{1,0:T(4,128)S(1)}, f32[768,4,64]{0,2,1:T(8,128)S(1)})) conditional(s32[]{:T(128)} %convert_element_type.100, (f32[4,768]{1,0:T(4,128)S(1)}, f32[4,768]{1,0:T(4,128)S(1)}, f32[768,4,64]{0,2,1:T(8,128)S(1)}) %tuple.41, (s32[]{:T(128)}, s32[]{:T(128)}, bf16[16,768,4,64]{1,3,2,0:T(8,128)(2,1)}, ...), branch_computations={%region_1.1_spmd, %region_2.4_spmd} | conditional | flops 649800192 | bytes 33734700 | solution.py:121
  187.6 0.7 iota_add_fusion
  188.6 3.9 fusion.4
  192.5 4.6 fusion.11
  197.1 3.5 fusion.3
  200.6 0.6 dynamic_slice.50
  201.9 0.6 dynamic_slice.50
  203.2 0.6 dynamic_slice.50
  204.5 0.6 dynamic_slice.50
  205.8 0.6 dynamic_slice.50
  207.0 0.6 dynamic_slice.50
  208.3 0.6 dynamic_slice.50
  209.6 0.6 dynamic_slice.50
  210.9 0.6 dynamic_slice.50
  212.2 0.6 dynamic_slice.50
  213.4 0.6 dynamic_slice.50
  214.7 0.6 dynamic_slice.50
  216.0 0.6 dynamic_slice.50
  218.5 0.6 dynamic_slice.50
  219.9 2.7 convolution_convert_fusion.1
  222.6 4.6 all-to-all-start.1
  227.4 38.2 %all-to-all-done.1 = bf16[8,96,2048]{2,1,0:T(8,128)(2,1)} async-done(((bf16[8,96,2048]{2,1,0:T(8,128)(2,1)}), bf16[8,96,2048]{2,1,0:T(8,128)(2,1)}, u32[]{:S(2)}, u32[]{:S(2)}) %all-to-all-start.1) | async-done | bytes 3145760 | tf_op jit(solution)/shard_map/all_to_all | solution.py:47
  265.6 2.5 reduce_sum.59
  268.1 1.2 fusion.35
  269.3 1.3 multiply_reduce_fusion.1
  270.7 2.0 add_convert_fusion.1
  272.7 5.3 copy.22
  278.0 215.4 %all-gather.8.cloned.1.call-done = bf16[768,2048]{1,0:T(8,128)(2,1)} async-done(((bf16[96,2048]{1,0:T(8,128)(2,1)}), bf16[768,2048]{1,0:T(8,128)(2,1)}) %all-gather.8.cloned.1.call-update) | async-done | bytes 3145744 | tf_op jit(solution)/shard_map/all_gather | solution.py:159
  493.4 6.5 %fusion.29 = f32[768,704]{0,1:T(8,128)} fusion(bf16[768,2048]{1,0:T(8,128)(2,1)} %all-gather.8.cloned.1.call-done, bf16[2048,1408]{0,1:T(8,128)(2,1)} %all-gather.10.cloned.1.call-done), kind=kOutput, calls=%fused_computation.33 | convolution fusion | flops 2214592512 | bytes 8192000 | tf_op jit(solution)/shard_map/dot_general | solution.py:161
  499.9 12.5 %convolution_convert_fusion = bf16[768,2048]{1,0:T(8,128)(2,1)} fusion(bf16[88,8,16,128]{3,2,1,0:T(8,128)(2,1)} %bitcast.52, f32[768,704]{0,1:T(8,128)} %fusion.29, bf16[768,2048]{1,0:T(8,128)(2,1)} %all-gather.8.cloned.1.call-done, bf16[2048,1408]{0,1:T(8,128)(2,1)} %all-gather.10.cloned.1.call-done), kind=kOutput, calls=%fused_computation.27 | convolution fusion | flops 4434001920 | bytes 14221312 | tf_op jit(solution)/shard_map/dot_general | solution.py:164
  512.5 36.1 %reduce-scatter.2.cloned.1.call-done = bf16[96,2048]{1,0:T(8,128)(2,1)} async-done(((bf16[768,2048]{1,0:T(8,128)(2,1)}), bf16[96,2048]{1,0:T(8,128)(2,1)}) %reduce-scatter.2.cloned.1.call-update) | async-done | bytes 393232 | tf_op jit(solution)/shard_map/reduce_scatter | solution.py:167
  548.6 1.2 fusion.36
  549.8 1.3 multiply_reduce_fusion
  551.1 2.0 add_convert_fusion
  (72 shorter events, 1.8 us)
Async XLA Ops:
  6.5 213.3 %copy-start = (bf16[256,2048]{1,0:T(8,128)(2,1)S(1)}, bf16[256,2048]{1,0:T(8,128)(2,1)}, u32[]{:S(2)}) copy-start(bf16[256,2048]{1,0:T(8,128)(2,1)} %param.22) | copy-start | bytes 3145732
  6.5 95.8 %all-gather.6.cloned.1.call-start = ((), (), s32[]{:S(2)}) async-start(), calls=%async_computation.3 | async-start | bytes 13369344 | tf_op jit(solution)/shard_map/all_gather | solution.py:37
  8.8 264.0 %all-gather.12.cloned.1.call-start = ((), (), s32[]{:S(2)}) async-start(), calls=%async_computation.7 | async-start | bytes 3063808 | tf_op jit(solution)/shard_map/all_gather | solution.py:11
  9.5 268.5 %all-gather.10.cloned.1.call-start = ((), (), s32[]{:S(2)}) async-start(), calls=%async_computation.5 | async-start | bytes 6127616 | tf_op jit(solution)/shard_map/all_gather | solution.py:37
  12.8 173.4 %all-to-all-start = ((f32[16,768,4]{1,2,0:T(4,128)}), f32[16,768,4]{1,2,0:T(4,128)S(1)}, u32[]{:S(2)}, u32[]{:S(2)}) async-start(f32[16,768,4]{1,2,0:T(4,128)} %broadcast_in_dim.56), calls=%async_computation | async-start | bytes 393216 | tf_op jit(solution)/shard_map/all_to_all | solution.py:24
  168.0 18.2 %copy-start.2 = (f32[768,4]{0,1:T(4,128)S(1)}, f32[768,4]{0,1:T(4,128)}, u32[]{:S(2)}) copy-start(f32[768,4]{0,1:T(4,128)} %param.20) | copy-start | bytes 36868
  222.6 48.0 %copy-start.3 = (f32[2048]{0:T(1024)S(1)}, f32[2048]{0:T(1024)}, u32[]{:S(2)}) copy-start(f32[2048]{0:T(1024)} %param.24) | copy-start | bytes 24580
  222.6 48.0 %copy-start.4 = (f32[2048]{0:T(1024)S(1)}, f32[2048]{0:T(1024)}, u32[]{:S(2)}) copy-start(f32[2048]{0:T(1024)} %param.23) | copy-start | bytes 24580
  222.6 43.0 %all-to-all-start.1 = ((bf16[8,96,2048]{2,1,0:T(8,128)(2,1)}), bf16[8,96,2048]{2,1,0:T(8,128)(2,1)}, u32[]{:S(2)}, u32[]{:S(2)}) async-start(bf16[8,96,2048]{2,1,0:T(8,128)(2,1)} %bitcast.50), calls=%async_computation.1 | async-start | bytes 6291456 | tf_op jit(solution)/shard_map/all_to_all | solution.py:47
  227.2 266.2 %all-gather.8.cloned.1.call-start = ((), (), s32[]{:S(2)}) async-start(), calls=%async_computation.4 | async-start | bytes 3538944 | tf_op jit(solution)/shard_map/all_gather | solution.py:159
  272.7 275.9 %reduce-scatter.2.cloned.1.call-start = ((), (), s32[]{:S(2)}) async-start(), calls=%async_computation.6 | async-start | bytes 3538944 | tf_op jit(solution)/shard_map/reduce_scatter | solution.py:167
  499.9 48.6 %copy-start.1 = (bf16[96,2048]{1,0:T(8,128)(2,1)S(1)}, bf16[96,2048]{1,0:T(8,128)(2,1)}, u32[]{:S(2)}) copy-start(bf16[96,2048]{1,0:T(8,128)(2,1)} %add_convert_fusion.1) | copy-start | bytes 1179652
  499.9 51.2 %copy-start.5 = (f32[2048]{0:T(1024)S(1)}, f32[2048]{0:T(1024)}, u32[]{:S(2)}) copy-start(f32[2048]{0:T(1024)} %param.29) | copy-start | bytes 24580
  499.9 51.2 %copy-start.6 = (f32[2048]{0:T(1024)S(1)}, f32[2048]{0:T(1024)}, u32[]{:S(2)}) copy-start(f32[2048]{0:T(1024)} %param.28) | copy-start | bytes 24580
Sparse Core Ops, SparseCore 0:
  9.5 92.8 all-gather.5
  104.5 46.6 all-gather.11
  153.3 63.4 all-gather.9
  272.8 220.5 all-gather.7
  512.6 35.9 reduce-scatter.1
